TPU v7x, 32 devices: a whole 2x2x4 slice. The times are simulated.
32 devices in a mesh: grp: 1, ep: 16 (over z, y, x), tp: 2 (over core).
Axes of the slice: x: 2, y: 2, z: 4, core: 2. Of those that a mesh axis runs over, the one named last changes fastest.
Arguments:
- tokens: bfloat16 [2048, 2048], P(('grp', 'ep', 'tp')), may hold values from -6 to 6
- norm_gain: float32 [2048], replicated, may hold values from 0.1 to 1.9
- expert_ids: int32 [2048, 2], P(('grp', 'ep', 'tp')), may hold values from 0 to 3, all different within a row; in each aligned block of 64 rows (0 to 63, 64 to 127, ...) at most 42 rows name the same one
- gate_weights: float32 [2048, 2], P(('grp', 'ep', 'tp')), may hold values from 0.2 to 1
- w_gate: bfloat16 [2048, 28672], P(None, ('ep', 'tp')), may hold values from -0.125 to 0.125
- w_up: bfloat16 [2048, 28672], P(None, ('ep', 'tp')), may hold values from -0.125 to 0.125
- w_down: bfloat16 [28672, 2048], P(('ep', 'tp')), may hold values from -0.0625 to 0.0625
Outputs:
- mixed: bfloat16 [2048, 2048], P(('grp', 'ep', 'tp'))
Inputs may be any that keep to these rules, and one draw needn't show every extreme that they name: `expert_ids`: each token names 2 different experts. Among the rows of one device no expert is named by more than 42 rows, a bound that some blocks reach; every expert is named somewhere.
All inputs are finite; a program needn't handle non-finite values.
Results may differ from a plain program's by a relative error of at most 0.0095.
Values may be sent and summed in bfloat16 or wider, within the bound.
A program may use at most 192 MiB of HBM per device.

v0:
```python
import jax
import jax.numpy as jnp
from jax import lax
from jax.sharding import PartitionSpec as P

GROUP = 4


def layer_norm(tokens, norm_gain):
    values = tokens.astype(jnp.float32)
    center = jnp.mean(values, -1, keepdims=True)
    spread = jnp.mean(jnp.square(values - center), -1, keepdims=True)
    return ((values - center) * lax.rsqrt(spread + 1e-05) * norm_gain).astype(jnp.bfloat16)


def rounded(values):
    return lax.optimization_barrier(values.astype(jnp.bfloat16)).astype(jnp.float32)


def per_device(tokens, norm_gain, expert_ids, gate_weights, w_gate, w_up, w_down):
    ep_devices = lax.axis_size("ep")
    local_rows, width = tokens.shape
    picks = expert_ids.shape[1]
    experts = ep_devices // GROUP
    capacity = max(2, min(local_rows, local_rows * picks * 4 // (3 * experts)))
    normed = layer_norm(tokens, norm_gain)
    flat_ids = expert_ids.reshape(-1)
    matches = (flat_ids[:, None] == jnp.arange(experts, dtype=jnp.int32)[None, :]).astype(jnp.int32)
    position = jnp.sum((jnp.cumsum(matches, 0) - 1) * matches, 1)
    target = flat_ids * capacity + position
    source = jnp.arange(local_rows * picks, dtype=jnp.int32) // picks
    packed = jnp.zeros((experts * capacity, width), jnp.bfloat16).at[target].set(normed[source])
    copies = jnp.broadcast_to(
        packed.reshape(experts, 1, capacity, width), (experts, GROUP, capacity, width)
    )
    copies = copies.reshape(ep_devices, capacity, width)
    arrived = lax.all_to_all(copies, "ep", split_axis=0, concat_axis=0, tiled=True).reshape(
        ep_devices * capacity, width
    )
    gate_all, up_all = (
        lax.all_gather(w_gate, "tp", axis=1, tiled=True),
        lax.all_gather(w_up, "tp", axis=1, tiled=True),
    )
    down_all = lax.all_gather(w_down, "tp", axis=0, tiled=True)
    gate_part = jnp.dot(arrived, gate_all, preferred_element_type=jnp.float32)
    up_part = jnp.dot(arrived, up_all, preferred_element_type=jnp.float32)
    hidden = (jax.nn.silu(gate_part) * up_part).astype(jnp.bfloat16)
    block_width = w_gate.shape[1]
    summed = jnp.zeros((ep_devices * capacity, width), jnp.float32)
    for side_index in range(lax.axis_size("tp")):
        lower = side_index * block_width
        summed = summed + rounded(
            jnp.dot(
                hidden[:, lower : lower + block_width],
                down_all[lower : lower + block_width],
                preferred_element_type=jnp.float32,
            )
        )
    partial_value = summed.astype(jnp.bfloat16).reshape(ep_devices, capacity, width)
    returned = lax.all_to_all(partial_value, "ep", split_axis=0, concat_axis=0, tiled=True)
    grouped = jnp.sum(returned.reshape(experts, GROUP, capacity, width).astype(jnp.float32), 1)
    grouped = grouped.reshape(experts * capacity, width)
    picked = grouped[target] * gate_weights.reshape(-1)[:, None]
    return jnp.sum(picked.reshape(local_rows, picks, width), 1).astype(jnp.bfloat16)


def solution(mesh):
    in_specs = (
        P(("grp", "ep", "tp"), None),
        P(),
        P(("grp", "ep", "tp"), None),
        P(("grp", "ep", "tp"), None),
        P(None, ("ep", "tp")),
        P(None, ("ep", "tp")),
        P(("ep", "tp"), None),
    )
    out_specs = P(("grp", "ep", "tp"), None)
    return jax.shard_map(
        per_device, mesh=mesh, in_specs=in_specs, out_specs=out_specs, check_vma=False
    )
```

profile of v0, /device:TPU:12, one launch (start us, length us, event | category | flops | bytes accessed | tf_op | source)
XLA Modules:
  0.0 217.5 jit_solution(18266885018147221790)
XLA Ops:
  6.5 0.7 all-gather.4.cloned.1.call-update
  7.3 0.7 all-gather.6.cloned.1.call-update
  9.1 0.2 fusion.14
  9.6 3.2 %scatter_custom_fusion = bf16[168,2048]{1,0:T(8,128)(2,1)S(1)} fusion(s32[128]{0:T(128)S(1)} %fusion.22, bf16[64,2048]{1,0:T(8,128)(2,1)S(1)} %fusion.16, s32[1024]{0:T(1024)S(1)} %pad_clamp_fusion.1, bf16[]{:T(256)} %constant.32.clone.1), kind=kCustom, calls=%fused_computation.22 | custom fusion | bytes 688130 | tf_op jit(solution)/shard_map/scatter | solution.py:32
  12.8 0.2 broadcast_in_dim.7
  13.0 2.0 broadcast_in_dim.8
  15.0 7.2 %all-to-all-start = ((bf16[16,42,2048]{2,1,0:T(8,128)(2,1)}), bf16[16,42,2048]{2,1,0:T(8,128)(2,1)S(1)}, u32[]{:S(2)}, u32[]{:S(2)}) async-start(bf16[16,42,2048]{2,1,0:T(8,128)(2,1)} %bitcast.16), calls=%async_computation | async-start | bytes 6291456 | tf_op jit(solution)/shard_map/all_to_all | solution.py:37
  22.2 0.2 all-gather.8.cloned.1.call-start
  22.4 0.5 all-gather.8.cloned.1.call-update
  22.9 69.8 %all-to-all-done = bf16[16,42,2048]{2,1,0:T(8,128)(2,1)S(1)} async-done(((bf16[16,42,2048]{2,1,0:T(8,128)(2,1)}), bf16[16,42,2048]{2,1,0:T(8,128)(2,1)S(1)}, u32[]{:S(2)}, u32[]{:S(2)}) %all-to-all-start) | async-done | bytes 2752544 | tf_op jit(solution)/shard_map/all_to_all | solution.py:37
  92.7 2.4 %reshape.112 = bf16[672,2048]{1,0:T(8,128)(2,1)} reshape(bf16[16,42,2048]{2,1,0:T(8,128)(2,1)S(1)} %all-to-all-done) | data formatting | bytes 5505024 | tf_op jit(solution)/shard_map/reshape | solution.py:37
  95.1 10.4 %fusion.23 = f32[672,1792]{1,0:T(8,128)} fusion(bf16[672,2048]{1,0:T(8,128)(2,1)} %reshape.112, bf16[2048,1792]{1,0:T(8,128)(2,1)} %all-gather.4.cloned.1.call-done), kind=kOutput, calls=%fused_computation.42 | convolution fusion | flops 4932501504 | bytes 14909440 | tf_op jit(solution)/shard_map/dot_general | solution.py:45
  105.6 10.3 %multiply_convert_fusion = bf16[672,1792]{1,0:T(8,128)(2,1)} fusion(f32[672,1792]{1,0:T(8,128)} %fusion.23, bf16[672,2048]{1,0:T(8,128)(2,1)S(1)} %copy-done, bf16[2048,1792]{1,0:T(8,128)(2,1)} %all-gather.6.cloned.1.call-done), kind=kOutput, calls=%fused_computation.5 | convolution fusion | flops 4939726848 | bytes 17317888 | tf_op jit(solution)/shard_map/dot_general | solution.py:46
  115.9 5.6 %fusion.4 = bf16[672,2048]{1,0:T(8,128)(2,1)S(1)} fusion(bf16[1792,2048]{1,0:T(8,128)(2,1)} %all-gather.8.cloned.1.call-done, bf16[672,1792]{1,0:T(8,128)(2,1)} %multiply_convert_fusion), kind=kOutput, calls=%fused_computation.10 | convolution fusion | flops 2467627008 | bytes 7626752 | tf_op jit(solution)/shard_map/dot_general | solution.py:53
  121.4 3.2 %fusion.7 = bf16[672,2048]{1,0:T(8,128)(2,1)S(1)} fusion(bf16[1792,2048]{1,0:T(8,128)(2,1)S(1)} %copy-done.5, bf16[672,1792]{1,0:T(8,128)(2,1)S(1)} %copy-done.6), kind=kOutput, calls=%fused_computation.11 | convolution fusion | flops 2467627008 | bytes 7626752 | tf_op jit(solution)/shard_map/dot_general | solution.py:53
  124.7 1.2 add_convert_fusion
  125.9 2.5 %reshape.113 = bf16[16,42,2048]{2,1,0:T(8,128)(2,1)} reshape(bf16[672,2048]{1,0:T(8,128)(2,1)S(1)} %add_convert_fusion) | data formatting | bytes 5505024 | tf_op jit(solution)/shard_map/reshape | solution.py:59
  128.3 5.6 %all-to-all-start.1 = ((bf16[16,42,2048]{2,1,0:T(8,128)(2,1)}), bf16[16,42,2048]{2,1,0:T(8,128)(2,1)S(1)}, u32[]{:S(2)}, u32[]{:S(2)}) async-start(bf16[16,42,2048]{2,1,0:T(8,128)(2,1)} %reshape.113), calls=%async_computation.1 | async-start | bytes 6291456 | tf_op jit(solution)/shard_map/all_to_all | solution.py:60
  134.0 69.8 %all-to-all-done.1 = bf16[16,42,2048]{2,1,0:T(8,128)(2,1)S(1)} async-done(((bf16[16,42,2048]{2,1,0:T(8,128)(2,1)}), bf16[16,42,2048]{2,1,0:T(8,128)(2,1)S(1)}, u32[]{:S(2)}, u32[]{:S(2)}) %all-to-all-start.1) | async-done | bytes 2752544 | tf_op jit(solution)/shard_map/all_to_all | solution.py:60
  203.8 1.7 convert_reduce_fusion
  205.6 1.6 reshape.114
  207.1 1.0 gather_fusion
  208.1 0.6 gather.10
  208.7 2.2 %multiply_reduce_fusion = bf16[64,2048]{1,0:T(8,128)(2,1)} fusion(f32[64,2,2048]{2,1,0:T(2,128)S(1)} %gather.10, f32[64,2]{1,0:T(8,128)S(1)} %copy.13), kind=kLoop, calls=%fused_computation.14 | loop fusion | flops 393216 | bytes 1311232 | tf_op jit(solution)/shard_map/reduce_sum | solution.py:64
  (36 shorter events, 1.4 us)
Async XLA Ops:
  6.5 1.5 copy-start.3
  6.5 2.4 %copy-start.1 = (bf16[64,2048]{1,0:T(8,128)(2,1)S(1)}, bf16[64,2048]{1,0:T(8,128)(2,1)}, u32[]{:S(2)}) copy-start(bf16[64,2048]{1,0:T(8,128)(2,1)} %param.7) | copy-start | bytes 786436
  6.5 2.8 %copy-start.2 = (f32[2048]{0:T(1024)S(1)}, f32[2048]{0:T(1024)}, u32[]{:S(2)}) copy-start(f32[2048]{0:T(1024)} %param.8) | copy-start | bytes 24580
  6.5 88.6 %all-gather.4.cloned.1.call-start = ((), (), s32[]{:S(2)}) async-start(), calls=%async_computation.2 | async-start | bytes 11010048 | tf_op jit(solution)/shard_map/all_gather | solution.py:41
  7.3 98.3 %all-gather.6.cloned.1.call-start = ((), (), s32[]{:S(2)}) async-start(), calls=%async_computation.3 | async-start | bytes 11010048 | tf_op jit(solution)/shard_map/all_gather | solution.py:42
  15.0 77.7 %all-to-all-start = ((bf16[16,42,2048]{2,1,0:T(8,128)(2,1)}), bf16[16,42,2048]{2,1,0:T(8,128)(2,1)S(1)}, u32[]{:S(2)}, u32[]{:S(2)}) async-start(bf16[16,42,2048]{2,1,0:T(8,128)(2,1)} %bitcast.16), calls=%async_computation | async-start | bytes 6291456 | tf_op jit(solution)/shard_map/all_to_all | solution.py:37
  22.2 93.7 %all-gather.8.cloned.1.call-start = ((), (), s32[]{:S(2)}) async-start(), calls=%async_computation.4 | async-start | bytes 11010048 | tf_op jit(solution)/shard_map/all_gather | solution.py:44
  95.1 10.5 %copy-start = (bf16[672,2048]{1,0:T(8,128)(2,1)S(1)}, bf16[672,2048]{1,0:T(8,128)(2,1)}, u32[]{:S(2)}) copy-start(bf16[672,2048]{1,0:T(8,128)(2,1)} %reshape.112) | copy-start | bytes 8257540
  115.9 5.6 %copy-start.6 = (bf16[672,1792]{1,0:T(8,128)(2,1)S(1)}, bf16[672,1792]{1,0:T(8,128)(2,1)}, u32[]{:S(2)}) copy-start(bf16[672,1792]{1,0:T(8,128)(2,1)} %multiply_convert_fusion) | copy-start | bytes 7225348
  115.9 5.6 %copy-start.5 = (bf16[1792,2048]{1,0:T(8,128)(2,1)S(1)}, bf16[1792,2048]{1,0:T(8,128)(2,1)}, u32[]{:S(2)}) copy-start(bf16[1792,2048]{1,0:T(8,128)(2,1)} %all-gather.8.cloned.1.call-done) | copy-start | bytes 22020100
  128.3 5.6 %copy-start.4 = (f32[64,2]{0,1:T(2,128)S(1)}, f32[64,2]{0,1:T(2,128)}, u32[]{:S(2)}) copy-start(f32[64,2]{0,1:T(2,128)} %param.10) | copy-start | bytes 1540
  128.3 75.5 %all-to-all-start.1 = ((bf16[16,42,2048]{2,1,0:T(8,128)(2,1)}), bf16[16,42,2048]{2,1,0:T(8,128)(2,1)S(1)}, u32[]{:S(2)}, u32[]{:S(2)}) async-start(bf16[16,42,2048]{2,1,0:T(8,128)(2,1)} %reshape.113), calls=%async_computation.1 | async-start | bytes 6291456 | tf_op jit(solution)/shard_map/all_to_all | solution.py:60
Sparse Core Ops, SparseCore 0:
  8.9 19.5 all-gather.3
  30.0 19.3 all-gather.5
  51.0 19.4 all-gather.7
where the time goes:
time: 218 us
  waiting for transfers between devices  142 us (65%)
  matrix products  29.5 us (14%)
  local copies, waits for them, and re-layouts  14 us (6%)
  between operations  13.3 us (6%)
  starting transfers between devices  13 us (6%)
  other arithmetic  6.16 us (3%)
    all_to_all x1, waiting for transfers between devices, per_device(): lax.all_to_all(copies, 'ep', split_axis=0, concat_axis=0, tiled=True)  69.8 us
    all_to_all x1, waiting for transfers between devices, per_device(): lax.all_to_all(partial_value, 'ep', split_axis=0, concat_axis=0, tiled=True)  69.8 us
    dot_general x1, matrix products, per_device(): gate_part = jnp.dot(arrived, gate_all, preferred_element_type=jnp.float32)  10.4 us
    dot_general x1, matrix products, per_device(): up_part = jnp.dot(arrived, up_all, preferred_element_type=jnp.float32)  10.3 us
    dot_general x2, matrix products, per_device(): jnp.dot(hidden[:, lower:lower + block_width], down_all[lower:lower + bloc...  8.8 us
    all_to_all x1, starting transfers between devices, per_device(): lax.all_to_all(copies, 'ep', split_axis=0, concat_axis=0, tiled=True)  7.17 us
    all_to_all x1, starting transfers between devices, per_device(): lax.all_to_all(partial_value, 'ep', split_axis=0, concat_axis=0, tiled=True)  5.57 us
  transfers between devices with their start and end apart: 5, of which 2 were waited for; matrix products, arithmetic and copies ran while one was open for 14% of the time, Pallas kernels for 0%

commit v1 on v0

v1 whole, which is shorter than its diff:
```python
import functools

import jax
import jax.numpy as jnp
from jax import lax
from jax.experimental import pallas as pl
from jax.experimental.pallas import tpu as pltpu
from jax.sharding import PartitionSpec as P

GROUP = 4
MESH = pl.DeviceIdType.MESH
F32, BF16 = jnp.float32, jnp.bfloat16
Z_IN, A_X, A_Y, R_X, R_Y, P_X0, P_X1, P_Y0, P_Y1, Q_X, Q_Y, Z_OUT = range(12)
COPIES = 12


def kernel(
    experts, cap, cols,
    tokens_ref, gain_ref, ids_ref, gates_ref, wg_ref, wu_ref, wd_ref, out_ref,
    wg, wu, wd, packed, xbuf, hidden, ybuf, rxa, rxb, cbuf, fbuf, zrx,
    send, recv, wsend, wrecv, wlocal,
):
    rows, width = tokens_ref.shape
    block = wg_ref.shape[1]
    half = width // 2
    grp, ep, core = lax.axis_index("grp"), lax.axis_index("ep"), lax.axis_index("tp")
    e, m = ep // GROUP, ep % GROUP
    left, right = pl.ds(0, half), pl.ds(half, half)

    def at(expert, member):
        return (grp, lax.rem(expert + 2 * experts, experts) * GROUP + member, core)

    mx = m + 1 - 2 * (m % 2)
    my = m + 2 - 4 * (m // 2)
    xdev, ydev = at(e, mx), at(e, my)
    other = (grp, ep, 1 - core)
    slots = experts * cap

    local = [
        pltpu.make_async_copy(wg_ref, wg.at[:, pl.ds(0, block)], wlocal.at[0]),
        pltpu.make_async_copy(wu_ref, wu.at[:, pl.ds(0, block)], wlocal.at[1]),
        pltpu.make_async_copy(wd_ref, wd.at[pl.ds(0, block)], wlocal.at[2]),
    ]
    for copy in local:
        copy.start()

    barrier = pltpu.get_barrier_semaphore()
    partners = [xdev, ydev, other] + [at(e - k, m) for k in range(1, experts)]
    for device in partners:
        pl.semaphore_signal(barrier, inc=1, device_id=device, device_id_type=MESH)

    values = tokens_ref[...].astype(F32)
    center = jnp.mean(values, -1, keepdims=True)
    spread = jnp.mean(jnp.square(values - center), -1, keepdims=True)
    normed = ((values - center) * lax.rsqrt(spread + 1e-05) * gain_ref[...]).astype(BF16)

    lane = lax.broadcasted_iota(jnp.int32, (rows, slots), 1)
    place = lane
    number = jnp.zeros((rows, slots), jnp.int32) + e
    for k in range(1, experts):
        past = (lane >= k * cap).astype(jnp.int32)
        place = place - cap * past
        number = number - past
    number = jnp.where(number < 0, number + experts, number)
    picks = ids_ref.shape[1]
    match = [(ids_ref[:, i : i + 1] == number).astype(F32) for i in range(picks)]
    named = functools.reduce(lambda a, b: a + b, match)
    before = (
        lax.broadcasted_iota(jnp.int32, (rows, rows), 1)
        < lax.broadcasted_iota(jnp.int32, (rows, rows), 0)
    ).astype(F32)
    position = jnp.dot(before.astype(BF16), named.astype(BF16), preferred_element_type=F32)
    taken = jnp.abs(position - place.astype(F32)) < 0.5
    chosen = [jnp.where(taken, one, 0.0).astype(BF16) for one in match]
    onehot = jnp.where(taken, named, 0.0)
    packed[...] = lax.dot_general(
        onehot.T.astype(BF16), normed, (((1,), (0,)), ((), ())), preferred_element_type=F32
    ).astype(BF16)
    xbuf[0, pl.ds(0, cap)] = packed[pl.ds(0, cap)]

    pl.semaphore_wait(barrier, len(partners))

    def remote(k, kind, src, dst, device):
        return pltpu.make_async_remote_copy(
            src_ref=src, dst_ref=dst, send_sem=send.at[k * COPIES + kind],
            recv_sem=recv.at[k * COPIES + kind], device_id=device, device_id_type=MESH,
        )

    def xs(k, j):
        return xbuf.at[k, pl.ds(j * cap, cap)]

    def ys(k, j, c):
        return ybuf.at[k, pl.ds(j * cap, cap), c]

    copies = {}
    for k in range(experts):
        if k:
            copies[k, Z_IN] = remote(k, Z_IN, packed.at[pl.ds(k * cap, cap)], xs(k, 0), at(e - k, m))
            copies[k, Z_OUT] = remote(k, Z_OUT, fbuf.at[k], zrx.at[pl.ds(k * cap, cap)], at(e + k, m))
        copies[k, A_X] = remote(k, A_X, xs(k, 0), xs(k, 1), xdev)
        copies[k, A_Y] = remote(k, A_Y, xs(k, 0), xs(k, 2), ydev)
        copies[k, R_Y] = remote(
            k, R_Y, xbuf.at[k, pl.ds(cap, cap), left], xbuf.at[k, pl.ds(3 * cap, cap), left], ydev)
        copies[k, R_X] = remote(
            k, R_X, xbuf.at[k, pl.ds(2 * cap, cap), right], xbuf.at[k, pl.ds(3 * cap, cap), right], xdev)
        copies[k, P_X0] = remote(k, P_X0, ys(k, 1, left), rxa.at[k, 0, :, left], xdev)
        copies[k, P_X1] = remote(k, P_X1, ys(k, 3, left), rxa.at[k, 1, :, left], xdev)
        copies[k, P_Y0] = remote(k, P_Y0, ys(k, 2, right), rxa.at[k, 0, :, right], ydev)
        copies[k, P_Y1] = remote(k, P_Y1, ys(k, 3, right), rxa.at[k, 1, :, right], ydev)
        copies[k, Q_Y] = remote(k, Q_Y, cbuf.at[k, :, left], rxb.at[k, :, left], ydev)
        copies[k, Q_X] = remote(k, Q_X, cbuf.at[k, :, right], rxb.at[k, :, right], xdev)

    def spread_out(k):
        if k:
            copies[k, Z_IN].wait_recv()
        copies[k, A_X].start()
        copies[k, A_Y].start()

    def relay(k):
        copies[k, A_X].wait_recv()
        copies[k, R_Y].start()
        copies[k, A_Y].wait_recv()
        copies[k, R_X].start()

    def compute(k):
        copies[k, R_Y].wait_recv()
        copies[k, R_X].wait_recv()

        def up(n, carry):
            at_n = pl.ds(pl.multiple_of(n * cols, cols), cols)
            x = xbuf[k]
            g = jnp.dot(x, wg[:, at_n], preferred_element_type=F32)
            u = jnp.dot(x, wu[:, at_n], preferred_element_type=F32)
            hidden[:, at_n] = (jax.nn.silu(g) * u).astype(BF16)
            return carry

        lax.fori_loop(0, 2 * block // cols, up, 0)

        def down(n, carry):
            at_n = pl.ds(pl.multiple_of(n * cols, cols), cols)
            ybuf[k, :, at_n] = jnp.dot(
                hidden[...], wd[:, at_n], preferred_element_type=F32
            ).astype(BF16)
            return carry

        lax.fori_loop(0, width // cols, down, 0)
        for kind in (P_X1, P_Y1, P_X0, P_Y0):
            copies[k, kind].start()

    def middle(k):
        copies[k, P_X1].wait_recv()
        cbuf[k, :, left] = (
            ybuf[k, pl.ds(2 * cap, cap), left].astype(F32) + rxa[k, 1, :, left].astype(F32)
        ).astype(BF16)
        copies[k, Q_Y].start()
        copies[k, P_Y1].wait_recv()
        cbuf[k, :, right] = (
            ybuf[k, pl.ds(cap, cap), right].astype(F32) + rxa[k, 1, :, right].astype(F32)
        ).astype(BF16)
        copies[k, Q_X].start()

    def finish(k):
        for kind in (P_X0, P_Y0, Q_X, Q_Y):
            copies[k, kind].wait_recv()
        total = (
            ybuf[k, pl.ds(0, cap)].astype(F32) + rxa[k, 0].astype(F32) + rxb[k].astype(F32)
        ).astype(BF16)
        if k:
            fbuf[k] = total
            copies[k, Z_OUT].start()
        else:
            zrx[pl.ds(0, cap)] = total

    for k in range(1, experts):
        copies[k, Z_IN].start()
    spread_out(0)
    weights = []
    for i, (src, dst) in enumerate(
        ((wg_ref, wg.at[:, pl.ds(block, block)]), (wu_ref, wu.at[:, pl.ds(block, block)]),
         (wd_ref, wd.at[pl.ds(block, block)]))
    ):
        weights.append(pltpu.make_async_remote_copy(
            src_ref=src, dst_ref=dst, send_sem=wsend.at[i], recv_sem=wrecv.at[i],
            device_id=other, device_id_type=MESH))
        weights[-1].start()
    for k in range(1, experts):
        spread_out(k)
        if k < experts - 1:
            relay(k - 1)
    for copy in local:
        copy.wait()
    for copy in weights:
        copy.wait_recv()
    for k in range(experts):
        compute(k)
        if k + experts - 2 < experts:
            relay(k + experts - 2)
        if k >= 1:
            middle(k - 1)
        if k >= 2:
            finish(k - 2)
    middle(experts - 1)
    finish(experts - 2)
    finish(experts - 1)

    for k in range(1, experts):
        copies[k, Z_OUT].wait_recv()

    def combine(n, carry):
        at_n = pl.ds(pl.multiple_of(n * cols, cols), cols)
        z = zrx[:, at_n]
        total = jnp.zeros((rows, cols), F32)
        for i in range(picks):
            total = total + gates_ref[:, i : i + 1] * jnp.dot(
                chosen[i], z, preferred_element_type=F32)
        out_ref[:, at_n] = total.astype(BF16)
        return carry

    lax.fori_loop(0, width // cols, combine, 0)
    for copy in copies.values():
        copy.wait_send()
    for copy in weights:
        copy.wait_send()


def per_device(tokens, norm_gain, expert_ids, gate_weights, w_gate, w_up, w_down):
    ep_devices = lax.axis_size("ep")
    rows, width = tokens.shape
    block = w_gate.shape[1]
    picks = expert_ids.shape[1]
    experts = ep_devices // GROUP
    capacity = max(2, min(rows, rows * picks * 4 // (3 * experts)))
    cap = -(-capacity // 16) * 16
    vmem = pl.BlockSpec(memory_space=pltpu.VMEM)
    hbm = pl.BlockSpec(memory_space=pl.ANY)
    chunk = GROUP * cap
    return pl.pallas_call(
        functools.partial(kernel, experts, cap, 256),
        out_shape=jax.ShapeDtypeStruct((rows, width), BF16),
        in_specs=[vmem] * 4 + [hbm] * 3,
        out_specs=vmem,
        scratch_shapes=[
            pltpu.VMEM((width, 2 * block), BF16),
            pltpu.VMEM((width, 2 * block), BF16),
            pltpu.VMEM((2 * block, width), BF16),
            pltpu.VMEM((experts * cap, width), BF16),
            pltpu.VMEM((experts, chunk, width), BF16),
            pltpu.VMEM((chunk, 2 * block), BF16),
            pltpu.VMEM((experts, chunk, width), BF16),
            pltpu.VMEM((experts, 2, cap, width), BF16),
            pltpu.VMEM((experts, cap, width), BF16),
            pltpu.VMEM((experts, cap, width), BF16),
            pltpu.VMEM((experts, cap, width), BF16),
            pltpu.VMEM((experts * cap, width), BF16),
            pltpu.SemaphoreType.DMA((experts * COPIES,)),
            pltpu.SemaphoreType.DMA((experts * COPIES,)),
            pltpu.SemaphoreType.DMA((3,)),
            pltpu.SemaphoreType.DMA((3,)),
            pltpu.SemaphoreType.DMA((3,)),
        ],
        compiler_params=pltpu.CompilerParams(
            collective_id=0, has_side_effects=True, vmem_limit_bytes=60 * 1024 * 1024),
    )(tokens, norm_gain.reshape(1, width), expert_ids, gate_weights, w_gate, w_up, w_down)


def solution(mesh):
    rows = P(("grp", "ep", "tp"), None)
    return jax.shard_map(
        per_device, mesh=mesh,
        in_specs=(rows, P(), rows, rows, P(None, ("ep", "tp")), P(None, ("ep", "tp")),
                  P(("ep", "tp"), None)),
        out_specs=rows, check_vma=False,
    )
```

time: 218 us -> 80 us (0.37)
  the two profiles are of different devices: /device:TPU:12 before, /device:TPU:0 now
where the time goes in v1:
time: 80 us; the launch traced here: 79.9 us
  Pallas kernels  75.4 us (94%)
  local copies, waits for them, and re-layouts  4.42 us (6%)
    pallas_call x1, Pallas kernels, per_device(): pl.pallas_call(functools.partial(kernel, experts, cap, 256), out_shape=ja...  75.4 us
    unnamed x3, local copies, waits for them, and re-layouts  4.42 us

profile of v1, /device:TPU:0, one launch (start us, length us, event | category | flops | bytes accessed | tf_op | source)
XLA Modules:
  0.0 79.9 jit_solution(1403198324773484261)
XLA Ops:
  0.0 1.4 %copy.8.ids_ref = s32[64,2]{1,0:T(8,128)} copy(s32[64,2]{0,1:T(2,128)} %param.9) | data formatting | bytes 1024 | tf_op args[2]
  1.4 1.4 %copy.9.gates_ref = f32[64,2]{1,0:T(8,128)} copy(f32[64,2]{0,1:T(2,128)} %param.10) | data formatting | bytes 1024 | tf_op args[3]
  2.7 75.4 %shard_map.73 = bf16[64,2048]{1,0:T(8,128)(2,1)} custom-call(bf16[64,2048]{1,0:T(8,128)(2,1)} %tokens_ref.1, f32[1,2048]{1,0:T(1,128)} %bitcast.1, s32[64,2]{1,0:T(8,128)} %copy.8.ids_ref, f32[64,2]{1,0:T(8,128)} %copy.9.gates_ref, bf16[2048,896]{1,0:T(8,128)(2,1)} %wg_ref.1, bf16[2048,896]{1,0:T(8,128)(2,1)} %wu_ref.1, bf16[896,2048]{1,0:T(8,128)(2,1)} %wd_ref.1), custom_call_target="tpu_custom_call" | custom-call | tf_op jit(solution)/shard_map/pallas_call | solution.py:237
  78.2 1.7 %copy.11 = bf16[64,2048]{1,0:T(8,128)(2,1)} copy(bf16[64,2048]{1,0:T(8,128)(2,1)} %shard_map.73) | data formatting | bytes 524288

commit v2 on v1

v2 whole, which is shorter than its diff:
```python
import functools

import jax
import jax.numpy as jnp
from jax import lax
from jax.experimental import pallas as pl
from jax.experimental.pallas import tpu as pltpu
from jax.sharding import PartitionSpec as P

GROUP = 4
MESH = pl.DeviceIdType.MESH
F32, BF16 = jnp.float32, jnp.bfloat16
Z_IN, A_X, A_Y, R_X, R_Y, P_X0, P_X1, P_Y0, P_Y1, Q_X, Q_Y, Z_OUT = range(12)
COPIES = 12


def kernel(
    experts, cap, cols,
    tokens_ref, gain_ref, ids_ref, gates_ref, wg_ref, wu_ref, wd_ref, out_ref,
    wg, wu, wd, packed, xbuf, hidden, ybuf, rxa, rxb, cbuf, fbuf, zrx,
    send, recv, wsend, wrecv, wlocal,
):
    rows, width = tokens_ref.shape
    block = wg_ref.shape[1]
    half = width // 2
    grp, ep, core = lax.axis_index("grp"), lax.axis_index("ep"), lax.axis_index("tp")
    e, m = ep // GROUP, ep % GROUP
    left, right = pl.ds(0, half), pl.ds(half, half)

    def at(expert, member):
        return (grp, expert * GROUP + member, core)

    edge = jnp.minimum(e, experts - 1 - e)
    toward = 1 - 2 * (e // (experts // 2))
    order = [e]
    for i in range(1, experts):
        paired = i <= 2 * edge
        step = (i + 1) // 2 if i % 2 else -(i // 2)
        order.append(jnp.where(paired, e + step, e + toward * (i - edge)))

    mx = m + 1 - 2 * (m % 2)
    my = m + 2 - 4 * (m // 2)
    xdev, ydev = at(e, mx), at(e, my)
    other = (grp, ep, 1 - core)
    slots = experts * cap

    local = [
        pltpu.make_async_copy(wg_ref, wg.at[:, pl.ds(0, block)], wlocal.at[0]),
        pltpu.make_async_copy(wu_ref, wu.at[:, pl.ds(0, block)], wlocal.at[1]),
        pltpu.make_async_copy(wd_ref, wd.at[pl.ds(0, block)], wlocal.at[2]),
    ]
    for copy in local:
        copy.start()

    barrier = pltpu.get_barrier_semaphore()
    partners = [xdev, ydev, other] + [at(plane, m) for plane in order[1:]]
    for device in partners:
        pl.semaphore_signal(barrier, inc=1, device_id=device, device_id_type=MESH)

    values = tokens_ref[...].astype(F32)
    center = jnp.mean(values, -1, keepdims=True)
    spread = jnp.mean(jnp.square(values - center), -1, keepdims=True)
    normed = ((values - center) * lax.rsqrt(spread + 1e-05) * gain_ref[...]).astype(BF16)

    row = lax.broadcasted_iota(jnp.int32, (slots, rows), 0)
    number = jnp.zeros((slots, rows), jnp.int32)
    for k in range(1, experts):
        number = number + (row >= k * cap).astype(jnp.int32)
    place = row - cap * number
    picks = ids_ref.shape[0]
    match = [(ids_ref[i : i + 1, :] == number).astype(F32) for i in range(picks)]
    named = functools.reduce(lambda a, b: a + b, match)
    before = (
        lax.broadcasted_iota(jnp.int32, (rows, rows), 0)
        < lax.broadcasted_iota(jnp.int32, (rows, rows), 1)
    ).astype(F32)
    position = jnp.dot(named.astype(BF16), before.astype(BF16), preferred_element_type=F32)
    taken = jnp.abs(position - place.astype(F32)) < 0.5
    chosen = [jnp.where(taken, one, 0.0) for one in match]
    gates = [
        jnp.sum((one * gates_ref[i : i + 1, :]).T, 1, keepdims=True)
        for i, one in enumerate(chosen)
    ]
    chosen = [one.T.astype(BF16) for one in chosen]
    onehot = jnp.where(taken, named, 0.0).astype(BF16)
    packed[...] = jnp.dot(onehot, normed, preferred_element_type=F32).astype(BF16)
    own = pl.ds(pl.multiple_of(e * cap, cap), cap)
    xbuf[e, pl.ds(0, cap)] = packed[own]

    pl.semaphore_wait(barrier, len(partners))

    turn = iter(range(2 * experts * COPIES))

    def remote(k, kind, src, dst, device):
        return pltpu.make_async_remote_copy(
            src_ref=src, dst_ref=dst, send_sem=send.at[next(turn)],
            recv_sem=recv.at[k * COPIES + kind], device_id=device, device_id_type=MESH,
        )

    def xs(k, j):
        return xbuf.at[k, pl.ds(j * cap, cap)]

    def ys(k, j, c):
        return ybuf.at[k, pl.ds(j * cap, cap), c]

    copies, arrivals = {}, {}
    for k in range(experts):
        k_ = order[k]
        if k:
            block_k = pl.ds(pl.multiple_of(k_ * cap, cap), cap)
            arrivals[k, Z_IN] = remote(k_, Z_IN, packed.at[block_k], xs(k_, 0), at(k_, m))
            copies[k, Z_IN] = remote(e, Z_IN, packed.at[block_k], xs(e, 0), at(k_, m))
            arrivals[k, Z_OUT] = remote(k_, Z_OUT, fbuf.at[k_], zrx.at[block_k], at(k_, m))
            copies[k, Z_OUT] = remote(e, Z_OUT, fbuf.at[k_], zrx.at[own], at(k_, m))
        copies[k, A_X] = remote(k_, A_X, xs(k_, 0), xs(k_, 1), xdev)
        copies[k, A_Y] = remote(k_, A_Y, xs(k_, 0), xs(k_, 2), ydev)
        copies[k, R_Y] = remote(k_, R_Y, xbuf.at[k_, pl.ds(cap, cap), left], xbuf.at[k_, pl.ds(3 * cap, cap), left], ydev)
        copies[k, R_X] = remote(k_, R_X, xbuf.at[k_, pl.ds(2 * cap, cap), right], xbuf.at[k_, pl.ds(3 * cap, cap), right], xdev)
        copies[k, P_X0] = remote(k_, P_X0, ys(k_, 1, left), rxa.at[k_, 0, :, left], xdev)
        copies[k, P_X1] = remote(k_, P_X1, ys(k_, 3, left), rxa.at[k_, 1, :, left], xdev)
        copies[k, P_Y0] = remote(k_, P_Y0, ys(k_, 2, right), rxa.at[k_, 0, :, right], ydev)
        copies[k, P_Y1] = remote(k_, P_Y1, ys(k_, 3, right), rxa.at[k_, 1, :, right], ydev)
        copies[k, Q_Y] = remote(k_, Q_Y, cbuf.at[k_, :, left], rxb.at[k_, :, left], ydev)
        copies[k, Q_X] = remote(k_, Q_X, cbuf.at[k_, :, right], rxb.at[k_, :, right], xdev)

    def spread_out(k):
        if k:
            arrivals[k, Z_IN].wait_recv()
        copies[k, A_X].start()
        copies[k, A_Y].start()

    def relay(k):
        copies[k, A_X].wait_recv()
        copies[k, R_Y].start()
        copies[k, A_Y].wait_recv()
        copies[k, R_X].start()

    def compute(k):
        k_ = order[k]
        copies[k, R_Y].wait_recv()
        copies[k, R_X].wait_recv()

        def up(n, carry):
            at_n = pl.ds(pl.multiple_of(n * cols, cols), cols)
            x = xbuf[k_]
            g = jnp.dot(x, wg[:, at_n], preferred_element_type=F32)
            u = jnp.dot(x, wu[:, at_n], preferred_element_type=F32)
            hidden[:, at_n] = (jax.nn.silu(g) * u).astype(BF16)
            return carry

        if k == turns[0]:
            for i in range(2):
                local[i].wait()
                weights[i].wait_recv()
        lax.fori_loop(0, 2 * block // cols, up, 0, unroll=True)
        if k == turns[0]:
            local[2].wait()
            weights[2].wait_recv()

        def down(n, carry):
            at_n = pl.ds(pl.multiple_of(n * cols, cols), cols)
            ybuf[k_, :, at_n] = jnp.dot(
                hidden[...], wd[:, at_n], preferred_element_type=F32
            ).astype(BF16)
            return carry

        lax.fori_loop(0, width // cols, down, 0, unroll=True)
        for kind in (P_X1, P_Y1, P_X0, P_Y0):
            copies[k, kind].start()

    def middle(k):
        k_ = order[k]
        copies[k, P_X1].wait_recv()
        cbuf[k_, :, left] = (
            ybuf[k_, pl.ds(2 * cap, cap), left].astype(F32) + rxa[k_, 1, :, left].astype(F32)
        ).astype(BF16)
        copies[k, Q_Y].start()
        copies[k, P_Y1].wait_recv()
        cbuf[k_, :, right] = (
            ybuf[k_, pl.ds(cap, cap), right].astype(F32) + rxa[k_, 1, :, right].astype(F32)
        ).astype(BF16)
        copies[k, Q_X].start()

    def finish(k):
        k_ = order[k]
        for kind in (P_X0, P_Y0, Q_X, Q_Y):
            copies[k, kind].wait_recv()
        total = (
            ybuf[k_, pl.ds(0, cap)].astype(F32) + rxa[k_, 0].astype(F32) + rxb[k_].astype(F32)
        ).astype(BF16)
        if k:
            fbuf[k_] = total
            copies[k, Z_OUT].start()
        else:
            zrx[own] = total

    for k in range(1, experts):
        copies[k, Z_IN].start()
    spread_out(0)
    weights = []
    for i, (src, dst) in enumerate(
        ((wg_ref, wg.at[:, pl.ds(block, block)]), (wu_ref, wu.at[:, pl.ds(block, block)]),
         (wd_ref, wd.at[pl.ds(block, block)]))
    ):
        weights.append(pltpu.make_async_remote_copy(
            src_ref=src, dst_ref=dst, send_sem=wsend.at[i], recv_sem=wrecv.at[i],
            device_id=other, device_id_type=MESH))
        weights[-1].start()
    turns = [*range(1, experts), 0]
    relay(0)
    for k in range(1, experts):
        spread_out(k)
        if k > 1:
            relay(k - 1)
    for i, k in enumerate(turns):
        compute(k)
        if i == 0:
            relay(experts - 1)
        if i >= 1:
            middle(turns[i - 1])
        if i >= 2:
            finish(turns[i - 2])
    middle(turns[-1])
    finish(turns[-2])
    finish(turns[-1])

    for k in range(1, experts):
        arrivals[k, Z_OUT].wait_recv()

    def combine(n, carry):
        at_n = pl.ds(pl.multiple_of(n * cols, cols), cols)
        z = zrx[:, at_n]
        total = jnp.zeros((rows, cols), F32)
        for i in range(picks):
            total = total + gates[i] * jnp.dot(
                chosen[i], z, preferred_element_type=F32)
        out_ref[:, at_n] = total.astype(BF16)
        return carry

    lax.fori_loop(0, width // cols, combine, 0)
    for copy in copies.values():
        copy.wait_send()
    for copy in weights:
        copy.wait_send()


def per_device(tokens, norm_gain, expert_ids, gate_weights, w_gate, w_up, w_down):
    ep_devices = lax.axis_size("ep")
    rows, width = tokens.shape
    block = w_gate.shape[1]
    picks = expert_ids.shape[1]
    experts = ep_devices // GROUP
    capacity = max(2, min(rows, rows * picks * 4 // (3 * experts)))
    cap = -(-capacity // 16) * 16
    vmem = pl.BlockSpec(memory_space=pltpu.VMEM)
    hbm = pl.BlockSpec(memory_space=pl.ANY)
    chunk = GROUP * cap
    return pl.pallas_call(
        functools.partial(kernel, experts, cap, 256),
        out_shape=jax.ShapeDtypeStruct((rows, width), BF16),
        in_specs=[vmem] * 4 + [hbm] * 3,
        out_specs=vmem,
        scratch_shapes=[
            pltpu.VMEM((width, 2 * block), BF16),
            pltpu.VMEM((width, 2 * block), BF16),
            pltpu.VMEM((2 * block, width), BF16),
            pltpu.VMEM((experts * cap, width), BF16),
            pltpu.VMEM((experts, chunk, width), BF16),
            pltpu.VMEM((chunk, 2 * block), BF16),
            pltpu.VMEM((experts, chunk, width), BF16),
            pltpu.VMEM((experts, 2, cap, width), BF16),
            pltpu.VMEM((experts, cap, width), BF16),
            pltpu.VMEM((experts, cap, width), BF16),
            pltpu.VMEM((experts, cap, width), BF16),
            pltpu.VMEM((experts * cap, width), BF16),
            pltpu.SemaphoreType.DMA((experts * (COPIES + 2),)),
            pltpu.SemaphoreType.DMA((experts * COPIES,)),
            pltpu.SemaphoreType.DMA((3,)),
            pltpu.SemaphoreType.DMA((3,)),
            pltpu.SemaphoreType.DMA((3,)),
        ],
        compiler_params=pltpu.CompilerParams(
            collective_id=0, has_side_effects=True, vmem_limit_bytes=60 * 1024 * 1024),
    )(tokens, norm_gain.reshape(1, width), expert_ids.T, gate_weights.T, w_gate, w_up, w_down)


def solution(mesh):
    rows = P(("grp", "ep", "tp"), None)
    return jax.shard_map(
        per_device, mesh=mesh,
        in_specs=(rows, P(), rows, rows, P(None, ("ep", "tp")), P(None, ("ep", "tp")),
                  P(("ep", "tp"), None)),
        out_specs=rows, check_vma=False,
    )
```

time: 80 us -> 75.4 us (0.943)
  local copies, waits for them, and re-layouts: 4.42 us -> 1.67 us
  Pallas kernels: 75.4 us -> 73.6 us
    unnamed x3 -> x1, local copies, waits for them, and re-layouts: 4.42 us -> 1.67 us
    pallas_call x1, Pallas kernels: 75.4 us -> 73.6 us  [per_device(): pl.pallas_call(functools.partial(kernel, experts, cap, 256), out_shape=ja...]
where the time goes in v2:
time: 75.4 us; the launch traced here: 75.3 us
  Pallas kernels  73.6 us (98%)
  local copies, waits for them, and re-layouts  1.67 us (2%)
    pallas_call x1, Pallas kernels, per_device(): pl.pallas_call(functools.partial(kernel, experts, cap, 256), out_shape=ja...  73.6 us
    unnamed x1, local copies, waits for them, and re-layouts  1.67 us

profile of v2, /device:TPU:0, one launch (start us, length us, event | category | flops | bytes accessed | tf_op | source)
XLA Modules:
  0.0 75.3 jit_solution(1649235737204236810)
XLA Ops:
  0.0 73.6 %shard_map.73 = bf16[64,2048]{1,0:T(8,128)(2,1)} custom-call(bf16[64,2048]{1,0:T(8,128)(2,1)} %tokens_ref.1, f32[1,2048]{1,0:T(1,128)} %bitcast.3, s32[2,64]{1,0:T(2,128)} %bitcast.4, f32[2,64]{1,0:T(2,128)} %bitcast.5, bf16[2048,896]{1,0:T(8,128)(2,1)} %wg_ref.1, bf16[2048,896]{1,0:T(8,128)(2,1)} %wu_ref.1, bf16[896,2048]{1,0:T(8,128)(2,1)} %wd_ref.1), custom_call_target="tpu_custom_call" | custom-call | tf_op jit(solution)/shard_map/pallas_call | solution.py:258
  73.6 1.7 %copy.9 = bf16[64,2048]{1,0:T(8,128)(2,1)} copy(bf16[64,2048]{1,0:T(8,128)(2,1)} %shard_map.73) | data formatting | bytes 524288
